TPU v7x, 32 devices: a whole 2x2x4 slice. The times are simulated.
32 devices in a mesh: grp: 2 (over y), sp: 8 (over z, core), tp: 2 (over x).
Axes of the slice: x: 2, y: 2, z: 4, core: 2. Of those that a mesh axis runs over, the one named last changes fastest.
Arguments:
- layer_input: bfloat16 [3072, 2048], P(('grp', 'sp', 'tp')), parts along dimension 0, may hold values from -6 to 6
- latent: bfloat16 [3072, 512], P(('grp', 'sp')), parts along dimension 0, may hold values from -6 to 6
- rope_key: bfloat16 [3072, 64], P(('grp', 'sp')), parts along dimension 0, may hold values from -4 to 4
- query_wide: bfloat16 [3072, 1536], P(('grp', 'sp'), 'tp'), parts along dimension 0, may hold values from -18 to 18
- query_narrow: bfloat16 [3072, 1024], P(('grp', 'sp'), 'tp'), parts along dimension 0, may hold values from -18 to 18
- key_up_wide: bfloat16 [512, 1024], P(None, 'tp'), may hold values from -0.25 to 0.25
- value_up_wide: bfloat16 [512, 1024], P(None, 'tp'), may hold values from -0.25 to 0.25
- key_up_narrow: bfloat16 [512, 512], P(None, 'tp'), may hold values from -0.25 to 0.25
- value_up_narrow: bfloat16 [512, 512], P(None, 'tp'), may hold values from -0.25 to 0.25
- out_wide: bfloat16 [1024, 2048], P('tp'), may hold values from -1.1953125 to 1.1953125
- out_narrow: bfloat16 [512, 2048], P('tp'), may hold values from -1.1953125 to 1.1953125
- norm_gain: float32 [2048], replicated, may hold values from 0.1 to 1.9
- gate_weight: bfloat16 [2048, 5632], P('sp', 'tp'), may hold values from -0.125 to 0.125
- value_weight: bfloat16 [2048, 5632], P('sp', 'tp'), may hold values from -0.125 to 0.125
- conv_weight: float32 [3, 5632], P(None, 'tp'), may hold values from -2.5 to 2.5
- down_weight: bfloat16 [5632, 2048], P('tp', 'sp'), may hold values from -0.078125 to 0.078125
Outputs:
- layer_output: bfloat16 [3072, 2048], P(('grp', 'sp', 'tp')), parts along dimension 0
There are 2 independent parts, one for each index of `grp`. A program takes and returns all parts, laid end to end along the dimension named above; an argument that names none is the same for every part. Nothing has to cross between parts.
All inputs are finite; a program needn't handle non-finite values.
Results may differ from a plain program's by a relative error of at most 0.015.
Values may be sent and summed in bfloat16 or wider, within the bound.
A program may use at most 128 MiB of HBM per device.

v0:
```python
import functools
import math

import jax
import jax.numpy as jnp
from jax import lax
from jax.experimental import pallas as pl
from jax.experimental.pallas import tpu as pltpu
from jax.sharding import PartitionSpec as P

NOPE_W = 128
NOPE_N = 64
LANES = 128
MESH = pl.DeviceIdType.MESH
BF = jnp.bfloat16
F32 = jnp.float32

rope_base = 10000.0
norm_eps = 1e-06


def cut_points(tiles, parts):
    plain = [k * tiles // parts for k in range(parts + 1)]
    even = [
        k * tiles // parts if 2 * k <= parts else tiles - (parts - k) * tiles // parts
        for k in range(parts + 1)
    ]

    def widest(cuts):
        return max(b - a for a, b in zip(cuts, cuts[1:]))

    return even if widest(even) <= widest(plain) else plain


def dot(a, b):
    return jnp.dot(a, b, preferred_element_type=F32)


def dot_t(a, b):
    return lax.dot_general(a, b, (((1,), (1,)), ((), ())), preferred_element_type=F32)


def layer_kernel(
    n,
    lat_in, qw, qn, gain, taps,
    x_in, kuw, kun, vuw, vun, ow, on, gate, value, down,
    out,
    lat, kuw_v, kun_v, vuw_v, vun_v, ow_v, xin_v,
    kw, kn, vw, vn, att, hpb, hrecv, mid,
    wg, wv, wd, xs, gp, vp, edge, halo, hid, pb, xr, zin,
    loc,
    lz_s, lz_r, lx_s, lx_r, lc_s, lc_r, lo_s, lo_r,
    wz_s, wz_r, wy_s, wy_r, wc_s, wc_r, wl,
    hx_s, hx_r, azr_s, azl_s, az_r, ax_s, ax_r, e_s, e_r,
    rx_s, rx_r, rz_s, rz_r,
):
    G, S, T = n["G"], n["S"], n["T"]
    Z = S // 2
    R = lat_in.shape[0]
    B = R // T
    LW = kuw.shape[0]
    D = xs.shape[3]
    HW, HN = qw.shape[0], qn.shape[0]
    WMAX = wg.shape[3]
    depth = gate.shape[0]
    cuts = cut_points(gate.shape[1] // LANES, Z)
    widths = [(b - a) * LANES for a, b in zip(cuts, cuts[1:])]
    g, s, t = lax.axis_index("grp"), lax.axis_index("sp"), lax.axis_index("tp")
    z, c = s // 2, s % 2

    def zdev(zz):
        return (g, 2 * zz + c, t)

    def xdev(tt):
        return (g, s, tt)

    sib = (g, 2 * z + 1 - c, t)
    xpart = [(t + d) % T for d in range(1, T)]
    if n["share"]:
        pb = xs

    def slot(sender, receiver):
        return (sender - receiver + T) % T - 1

    ypart = [(g + d) % G for d in range(1, G)]

    def rcopy(src, dst, ss, rs, dev):
        return pltpu.make_async_remote_copy(
            src_ref=src, dst_ref=dst, send_sem=ss, recv_sem=rs, device_id=dev, device_id_type=MESH
        )

    def got(ref, rs):
        rcopy(ref, ref, rs, rs, sib).wait_recv()

    def sent(ref, ss):
        rcopy(ref, ref, ss, ss, sib).wait_send()

    def rows(part):
        return pl.ds(pl.multiple_of(part * B, B), B)

    bar = pltpu.get_barrier_semaphore()
    for zz in range(Z):
        @pl.when(zz != z)
        def _():
            pl.semaphore_signal(bar, inc=1, device_id=zdev(zz), device_id_type=MESH)
    for tt in xpart:
        pl.semaphore_signal(bar, inc=1, device_id=xdev(tt), device_id_type=MESH)
    for gg in ypart:
        pl.semaphore_signal(bar, inc=1, device_id=(gg, s, t), device_id_type=MESH)
    pl.semaphore_signal(bar, inc=1, device_id=sib, device_id_type=MESH)
    pl.semaphore_wait(bar, Z + T + G - 2)

    for zz in range(Z):
        @pl.when(zz != z)
        def _():
            rcopy(lat_in.at[rows(t)], lat.at[s, rows(t)], lz_s.at[zz], lz_r.at[z], zdev(zz)).start()
    rcopy(lat_in, lat.at[s], lo_s, lo_r, sib).start()

    mats = ((gate, wg), (value, wv), (down, wd))
    hd = depth // G

    def piece(ai, zz, cc, gg, w):
        if ai < 2:
            return mats[ai][1].at[zz, cc, pl.ds(pl.multiple_of(gg * hd, hd), hd), pl.ds(0, w)]
        wh = w // G
        return wd.at[zz, cc, pl.ds(pl.multiple_of(gg * wh, wh), wh)]

    def slab(ai, cc, w):
        if ai < 2:
            return mats[ai][1].at[:, cc, :, pl.ds(0, w)]
        return wd.at[:, cc, pl.ds(0, w)]

    def own_copy(ai, zz):
        w, lo = widths[zz], cuts[zz] * LANES
        if ai < 2:
            return pltpu.make_async_copy(
                mats[ai][0].at[:, pl.ds(lo, w)], mats[ai][1].at[zz, c, :, pl.ds(0, w)], wl.at[ai]
            )
        return pltpu.make_async_copy(down.at[pl.ds(lo, w)], wd.at[zz, c, pl.ds(0, w)], wl.at[ai])

    def hbm_piece(ai, zz):
        w, lo = widths[zz], cuts[zz] * LANES
        if ai < 2:
            return mats[ai][0].at[pl.ds(pl.multiple_of(g * hd, hd), hd), pl.ds(lo, w)]
        wh = w // G
        return down.at[pl.ds(pl.multiple_of(lo + g * wh, math.gcd(lo, wh) if lo else wh), wh)]

    def spread(ai):
        for zz in range(Z):
            if widths[zz]:
                @pl.when(zz != z)
                def _():
                    rcopy(
                        hbm_piece(ai, zz), piece(ai, z, c, g, widths[zz]),
                        wz_s.at[ai, zz], wz_r.at[ai, z], zdev(zz),
                    ).start()

                @pl.when(zz == z)
                def _():
                    own_copy(ai, zz).start()

    def by_width(body):
        for w in sorted(set(widths)):
            mine = functools.reduce(
                jnp.logical_or, [z == k for k in range(Z) if widths[k] == w]
            )

            @pl.when(mine)
            def _():
                body(w)

    def relay_y(ai):
        def body(w):
            if not w:
                return
            for zz in range(Z):
                @pl.when(zz != z)
                def _():
                    part = piece(ai, zz, c, g, w)
                    got(part, wz_r.at[ai, zz])
                    for gg in ypart:
                        rcopy(part, part, wy_s.at[ai, zz, gg], wy_r.at[ai, zz, g], (gg, s, t)).start()
        by_width(body)

    def relay_core(ai):
        def body(w):
            if not w:
                return
            for zz in range(Z):
                if widths[zz] == w:
                    @pl.when(zz == z)
                    def _():
                        own_copy(ai, zz).wait()
            for zz in range(Z):
                @pl.when(zz != z)
                def _():
                    for gg in ypart:
                        got(piece(ai, zz, c, gg, w), wy_r.at[ai, zz, gg])
            rcopy(slab(ai, c, w), slab(ai, c, w), wc_s.at[ai], wc_r.at[ai], sib).start()
        by_width(body)

    def arrive(ai):
        def body(w):
            if w:
                got(slab(ai, 1 - c, w), wc_r.at[ai])
        by_width(body)

    def spread_sent(ai):
        for zz in range(Z):
            if widths[zz]:
                @pl.when(zz != z)
                def _():
                    sent(hbm_piece(ai, zz), wz_s.at[ai, zz])

        def body(w):
            if not w:
                return
            for zz in range(Z):
                @pl.when(zz != z)
                def _():
                    for gg in ypart:
                        sent(piece(ai, zz, c, g, w), wy_s.at[ai, zz, gg])
            sent(slab(ai, c, w), wc_s.at[ai])
        by_width(body)

    for ai in range(3):
        spread(ai)

    half = NOPE_N
    local = [
        pltpu.make_async_copy(kuw, kuw_v, loc.at[0]),
        pltpu.make_async_copy(kun, kun_v, loc.at[1]),
        pltpu.make_async_copy(vuw, vuw_v, loc.at[2]),
        pltpu.make_async_copy(vun, vun_v, loc.at[3]),
        pltpu.make_async_copy(x_in, xin_v, loc.at[4]),
        pltpu.make_async_copy(ow, ow_v.at[pl.ds(0, HW * LANES)], loc.at[5]),
    ]
    for h in range(HN):
        local.append(
            pltpu.make_async_copy(
                on.at[pl.ds(h * half, half)],
                ow_v.at[pl.ds((HW + h) * LANES, half)],
                loc.at[6 + h],
            )
        )
    for cp in local:
        cp.start()
    for h in range(HN):
        ow_v[pl.ds((HW + h) * LANES + half, LANES - half), :] = jnp.zeros((LANES - half, D), BF)

    def clear(w):
        if w < WMAX:
            gap = WMAX - w
            for ref in (wg, wv):
                ref[:, :, :, pl.ds(w, gap)] = jnp.zeros((Z, 2, depth, gap), BF)
            wd[:, :, pl.ds(w, gap), :] = jnp.zeros((Z, 2, gap, wd.shape[3]), BF)
    by_width(clear)

    lat[s] = lat_in[...]
    for cp in local[:4]:
        cp.wait()

    for zz in range(Z):
        @pl.when(zz != z)
        def _():
            part = lat.at[2 * zz + c, rows(t)]
            got(part, lz_r.at[zz])
            for tt in xpart:
                rcopy(part, part, lx_s.at[zz, tt], lx_r.at[zz, t], xdev(tt)).start()
            rcopy(part, part, lc_s.at[zz, t], lc_r.at[zz, t], sib).start()
    for zz in range(Z):
        @pl.when(zz != z)
        def _():
            for tt in xpart:
                part = lat.at[2 * zz + c, rows(tt)]
                got(part, lx_r.at[zz, tt])
                rcopy(part, part, lc_s.at[zz, tt], lc_r.at[zz, tt], sib).start()
    got(lat.at[2 * z + 1 - c], lo_r)
    for zz in range(Z):
        @pl.when(zz != z)
        def _():
            for tt in range(T):
                got(lat.at[2 * zz + 1 - c, rows(tt)], lc_r.at[zz, tt])

    def expand(i, carry):
        at = pl.ds(pl.multiple_of(i * R, R), R)
        low = lat[i, :, pl.ds(0, LW)]
        turned = lat[i, :, pl.ds(LW, LANES)]
        key = dot(low, kuw_v[...]).astype(BF)
        val = dot(low, vuw_v[...]).astype(BF)
        for h in range(HW):
            kw[h, at, pl.ds(0, LANES)] = key[:, h * LANES : (h + 1) * LANES]
            kw[h, at, pl.ds(LANES, LANES)] = turned
            vw[h, at, :] = val[:, h * LANES : (h + 1) * LANES]
        key = dot(low, kun_v[...]).astype(BF)
        val = dot(low, vun_v[...]).astype(BF)
        for h in range(HN):
            kn[h, at, :] = key[:, h * LANES : (h + 1) * LANES] + turned
            vn[h, at, :] = val[:, h * LANES : (h + 1) * LANES]
        return carry

    lax.fori_loop(0, S, expand, 0)

    def heads(q, k, v, count, first, scale):
        def body(h, carry):
            score = dot_t(q[h], k[h]) * (scale * math.log2(math.e))
            prob = jnp.exp2(score - jnp.max(score, axis=-1, keepdims=True))
            total = jnp.sum(prob, axis=-1, keepdims=True)
            mixed = dot(prob.astype(BF), v[h]) / total
            at = pl.ds(pl.multiple_of((first + h) * LANES, LANES), LANES)
            att[:, at] = mixed.astype(BF)
            return carry

        lax.fori_loop(0, count, body, 0)

    heads(qw, kw, vw, HW, 0, n["scale_w"])
    relay_y(0)
    heads(qn, kn, vn, HN, HW, n["scale_n"])

    for cp in local[4:]:
        cp.wait()
    NB = n["NB"]
    cw = D // NB
    for j in range(NB):
        cols = pl.ds(j * cw, cw)
        hpb[:, cols] = dot(att[...], ow_v[:, cols]).astype(BF)
        for tt in xpart:
            rcopy(
                hpb.at[rows(tt), cols], hrecv.at[t, :, cols], hx_s.at[tt, j], hx_r.at[t, j], xdev(tt)
            ).start()
    for j in range(NB):
        cols = pl.ds(j * cw, cw)
        part = hpb[rows(t), cols].astype(F32)
        for tt in xpart:
            got(hrecv.at[tt, :, cols], hx_r.at[tt, j])
            part = part + hrecv[tt, :, cols].astype(F32)
        mid[:, cols] = (xin_v[:, cols].astype(F32) + part).astype(BF).astype(F32)
    full = mid[...]
    power = jnp.mean(full * full, axis=-1, keepdims=True)
    xs[z, t] = (full * lax.rsqrt(power + norm_eps) * gain[...]).astype(BF)

    def forward(zi):
        blk = xs.at[zi, t]

        @pl.when((zi <= z) & (z < Z - 1))
        def _():
            rcopy(blk, blk, azr_s.at[zi], az_r.at[zi], zdev(z + 1)).start()

        @pl.when((zi >= z) & (z > 0))
        def _():
            rcopy(blk, blk, azl_s.at[zi], az_r.at[zi], zdev(z - 1)).start()
        for tt in xpart:
            rcopy(blk, blk, ax_s.at[zi, tt], ax_r.at[zi, t], xdev(tt)).start()

    def rows_sent():
        for zz in range(Z):
            @pl.when((zz <= z) & (z < Z - 1))
            def _():
                sent(xs.at[zz, t], azr_s.at[zz])

            @pl.when((zz >= z) & (z > 0))
            def _():
                sent(xs.at[zz, t], azl_s.at[zz])
            for tt in xpart:
                sent(xs.at[zz, t], ax_s.at[zz, tt])

    near = jnp.minimum(z, Z - 1 - z)
    outward = jnp.where(z < Z - 1 - z, 1, -1)

    def order(i):
        sign = jnp.where(i % 2 == 1, 1, -1)
        return jnp.where(i <= 2 * near, z + sign * ((i + 1) // 2), z + outward * (i - near))

    forward(z)
    relay_y(1)
    relay_core(0)
    relay_y(2)
    arrive(0)
    relay_core(1)
    arrive(1)

    NC = WMAX // n["NW"]

    def project(i, carry):
        zi = order(i)

        @pl.when(i + 1 < Z)
        def _():
            nxt = order(i + 1)
            got(xs.at[nxt, t], az_r.at[nxt])
            forward(nxt)
        for tt in xpart:
            got(xs.at[zi, tt], ax_r.at[zi, tt])
        block = xs[zi].reshape(R, D)
        for j in range(n["NW"]):
            cols = pl.ds(j * NC, NC)
            pre = dot(block, wg[:, :, :, cols].reshape(D, NC)).astype(BF)
            gp[zi, :, cols] = pre
            edge[zi, pl.ds(0, 8), cols] = pre[:8].astype(F32)
            edge[zi, pl.ds(8, 8), cols] = pre[R - 8 :].astype(F32)
        for j in range(n["NW"]):
            cols = pl.ds(j * NC, NC)
            vp[zi, :, cols] = dot(block, wv[:, :, :, cols].reshape(D, NC))
        return carry

    lax.fori_loop(0, Z, project, 0)
    rcopy(edge, halo, e_s, e_r, sib).start()
    relay_core(2)
    arrive(2)
    got(halo, e_r)
    if n["share"]:
        rows_sent()

    place = lax.broadcasted_iota(jnp.int32, (R, NC), 0)
    OW = wd.shape[3]

    def add_up(zi):
        total = pb[zi, t].astype(F32)
        for tt in xpart:
            part = xr.at[zi, slot(tt, t)]
            got(part, rx_r.at[zi, tt])
            total = total + part[...].astype(F32)
        inner = ((zi > z) & (z > 0)) | ((zi < z) & (z < Z - 1))

        @pl.when(inner)
        def _():
            got(zin.at[zi], rz_r.at[zi])
            pb[zi, t] = (total + zin[zi].astype(F32)).astype(BF)

        @pl.when(jnp.logical_not(inner))
        def _():
            pb[zi, t] = total.astype(BF)

        @pl.when(zi > z)
        def _():
            rcopy(pb.at[zi, t], zin.at[zi], rz_s.at[zi], rz_r.at[zi], zdev(z + 1)).start()

        @pl.when(zi < z)
        def _():
            into = jnp.where(zi == z - 1, Z, zi)
            rcopy(pb.at[zi, t], zin.at[into], rz_s.at[zi], rz_r.at[into], zdev(z - 1)).start()

    def mix(k, carry):
        zi = order(Z - 1 - k)
        above, below = zi - 1 + c, zi + c
        has_above = jnp.where(above >= 0, 1.0, 0.0)
        has_below = jnp.where(below < Z, 1.0, 0.0)
        above, below = jnp.maximum(above, 0), jnp.minimum(below, Z - 1)
        for j in range(n["NW"]):
            cols = pl.ds(j * NC, NC)
            pre = gp[zi, :, cols].astype(F32)
            prev = halo[above, pl.ds(8, 8), cols][7:8] * has_above
            post = halo[below, pl.ds(0, 8), cols][0:1] * has_below
            up = jnp.where(place == 0, prev, pltpu.roll(pre, 1, 0))
            dn = jnp.where(place == R - 1, post, pltpu.roll(pre, R - 1, 0))
            conv = taps[0:1, cols] * up + taps[1:2, cols] * pre + taps[2:3, cols] * dn
            hid[:, cols] = (conv / (1.0 + jnp.exp(-conv)) * vp[zi, :, cols]).astype(BF)
        for zz in range(Z):
            for cc in range(2):
                part = dot(hid[...], wd[zz, cc]).astype(BF)
                pb[zi, :, :, pl.ds((2 * zz + cc) * OW, OW)] = part.reshape(T, B, OW)
        for tt in xpart:
            rcopy(pb.at[zi, tt], xr.at[zi, slot(t, tt)], rx_s.at[zi, tt], rx_r.at[zi, t], xdev(tt)).start()

        @pl.when(k > 0)
        def _():
            add_up(order(Z - k))
        return carry

    lax.fori_loop(0, Z, mix, 0)
    total = pb[z, t].astype(F32)
    for tt in xpart:
        part = xr.at[z, slot(tt, t)]
        got(part, rx_r.at[z, tt])
        total = total + part[...].astype(F32)
    mid[...] = mid[...] + total

    @pl.when(z > 0)
    def _():
        got(zin.at[z], rz_r.at[z])
        mid[...] = mid[...] + zin[z].astype(F32)

    @pl.when(z < Z - 1)
    def _():
        got(zin.at[Z], rz_r.at[Z])
        mid[...] = mid[...] + zin[Z].astype(F32)
    out[...] = mid[...].astype(BF)

    sent(lat_in, lo_s)
    sent(edge, e_s)
    for ai in range(3):
        spread_sent(ai)
    for tt in xpart:
        for j in range(NB):
            sent(hpb.at[rows(tt), pl.ds(j * cw, cw)], hx_s.at[tt, j])
    for zz in range(Z):
        @pl.when(zz != z)
        def _():
            part = lat.at[2 * zz + c, rows(t)]
            sent(part, lz_s.at[zz])
            for tt in xpart:
                sent(part, lx_s.at[zz, tt])
            for tt in range(T):
                sent(part, lc_s.at[zz, tt])
            sent(pb.at[zz, t], rz_s.at[zz])
        for tt in xpart:
            sent(pb.at[zz, tt], rx_s.at[zz, tt])
    if not n["share"]:
        rows_sent()


def rope_tables(row_start, row_total, span_width):
    places = (row_start + jnp.arange(row_total, dtype=jnp.int32)).astype(F32)
    frequency = jnp.power(
        rope_base, -jnp.arange(0, span_width, 2, dtype=jnp.int32).astype(F32) / span_width
    )
    angles = places[:, None] * frequency[None, :]
    angles = jnp.concatenate([angles, angles], axis=-1)
    return (jnp.cos(angles), jnp.sin(angles))


def spin_rows(entries, cosine, sine_table):
    entries = entries.astype(F32)
    lead_half, tail_half = jnp.split(entries, 2, axis=-1)
    return entries * cosine + jnp.concatenate([-tail_half, lead_half], axis=-1) * sine_table


def split_queries(queries, heads, nope, cosine, sine_table):
    shaped = queries.reshape(queries.shape[0], heads, -1)
    turned = spin_rows(shaped[:, :, nope:], cosine[:, None, :], sine_table[:, None, :]).astype(BF)
    return shaped[:, :, :nope], turned


def layer(
    layer_input,
    latent,
    rope_key,
    query_wide,
    query_narrow,
    key_up_wide,
    value_up_wide,
    key_up_narrow,
    value_up_narrow,
    out_wide,
    out_narrow,
    norm_gain,
    gate_weight,
    value_weight,
    conv_weight,
    down_weight,
):
    G, S, T = lax.axis_size("grp"), lax.axis_size("sp"), lax.axis_size("tp")
    Z = S // 2
    R, LW = latent.shape
    rot = rope_key.shape[1]
    D = layer_input.shape[1]
    B = R // T
    HW = key_up_wide.shape[1] // NOPE_W
    HN = key_up_narrow.shape[1] // NOPE_N
    cosine, sine_table = rope_tables(lax.axis_index("sp") * R, R, rot)
    turned_key = spin_rows(rope_key, cosine, sine_table).astype(BF)
    lat = jnp.concatenate([latent, turned_key, jnp.zeros((R, LANES - rot), BF)], axis=1)
    nope, turned = split_queries(query_wide, HW, NOPE_W, cosine, sine_table)
    qw = jnp.concatenate([nope, turned, jnp.zeros((R, HW, LANES - rot), BF)], axis=2)
    nope, turned = split_queries(query_narrow, HN, NOPE_N, cosine, sine_table)
    qn = jnp.concatenate([turned, nope], axis=2)
    qw, qn = qw.transpose(1, 0, 2), qn.transpose(1, 0, 2)
    pad_key = jnp.pad(
        key_up_narrow.reshape(LW, HN, NOPE_N), ((0, 0), (0, 0), (LANES - NOPE_N, 0))
    ).reshape(LW, HN * LANES)
    pad_value = jnp.pad(
        value_up_narrow.reshape(LW, HN, NOPE_N), ((0, 0), (0, 0), (0, LANES - NOPE_N))
    ).reshape(LW, HN * LANES)
    tiles = gate_weight.shape[1] // LANES
    cuts = cut_points(tiles, Z)
    wmax = max(b - a for a, b in zip(cuts, cuts[1:])) * LANES
    start = jnp.asarray(cuts, jnp.int32)[lax.axis_index("sp") // 2] * LANES
    taps = lax.dynamic_slice_in_dim(
        jnp.pad(conv_weight, ((0, 0), (0, wmax))), start, wmax, axis=1
    )
    keys = S * R
    depth, ow = gate_weight.shape[0], down_weight.shape[1]
    share = Z * T * B * D * 2 > 8 << 20
    n = dict(
        share=share,
        G=G,
        S=S,
        T=T,
        NB=4,
        NW=max(1, wmax // 256),
        scale_w=1.0 / math.sqrt(NOPE_W + rot),
        scale_n=1.0 / math.sqrt(NOPE_N + rot),
    )
    vmem = pl.BlockSpec(memory_space=pltpu.VMEM)
    hbm = pl.BlockSpec(memory_space=pl.ANY)

    def V(*shape, dtype=BF):
        return pltpu.VMEM(shape, dtype)

    def sem(*shape):
        return pltpu.SemaphoreType.DMA(shape)

    one = pltpu.SemaphoreType.DMA
    scratch = [
        V(S, R, lat.shape[1]),
        V(LW, HW * LANES), V(LW, HN * LANES), V(LW, HW * LANES), V(LW, HN * LANES),
        V((HW + HN) * LANES, D), V(B, D),
        V(HW, keys, 2 * LANES), V(HN, keys, LANES), V(HW, keys, LANES), V(HN, keys, LANES),
        V(R, (HW + HN) * LANES), V(R, D), V(T, B, D), V(B, D, dtype=F32),
        V(Z, 2, depth, wmax), V(Z, 2, depth, wmax), V(Z, 2, wmax, ow),
        V(Z, T, B, D), V(Z, R, wmax), V(Z, R, wmax, dtype=F32),
        V(Z, 16, wmax, dtype=F32), V(Z, 16, wmax, dtype=F32), V(R, wmax),
        V(8, LANES) if share else V(Z, T, B, D), V(Z, T - 1, B, D), V(Z + 1, B, D),
        sem(6 + HN),
        sem(Z), sem(Z), sem(Z, T), sem(Z, T), sem(Z, T), sem(Z, T), one, one,
        sem(3, Z), sem(3, Z), sem(3, Z, G), sem(3, Z, G), sem(3), sem(3), sem(3),
        sem(T, 4), sem(T, 4), sem(Z), sem(Z), sem(Z), sem(Z, T), sem(Z, T), one, one,
        sem(Z, T), sem(Z, T), sem(Z), sem(Z + 1),
    ]
    return pl.pallas_call(
        functools.partial(layer_kernel, n),
        out_shape=jax.ShapeDtypeStruct((B, D), BF),
        in_specs=[vmem] * 5 + [hbm] * 10,
        out_specs=vmem,
        scratch_shapes=scratch,
        compiler_params=pltpu.CompilerParams(
            collective_id=0, has_side_effects=True, vmem_limit_bytes=63 << 20
        ),
        name="layer",
    )(
        lat, qw, qn, norm_gain.reshape(1, D), taps,
        layer_input, key_up_wide, pad_key, value_up_wide, pad_value, out_wide, out_narrow,
        gate_weight, value_weight, down_weight,
    )


def solution(mesh):
    in_specs = (
        P(("grp", "sp", "tp"), None),
        P(("grp", "sp"), None),
        P(("grp", "sp"), None),
        P(("grp", "sp"), "tp"),
        P(("grp", "sp"), "tp"),
        P(None, "tp"),
        P(None, "tp"),
        P(None, "tp"),
        P(None, "tp"),
        P("tp", None),
        P("tp", None),
        P(),
        P("sp", "tp"),
        P("sp", "tp"),
        P(None, "tp"),
        P("tp", "sp"),
    )
    out_specs = P(("grp", "sp", "tp"), None)
    return jax.shard_map(
        layer, mesh=mesh, in_specs=in_specs, out_specs=out_specs, check_vma=False
    )
```

profile of v0, /device:TPU:16, one launch (start us, length us, event | category | flops | bytes accessed | tf_op | source)
XLA Modules:
  0.0 164.8 jit_solution(16788774531287007756)
XLA Ops:
  0.0 0.0 copy-start.3
  0.0 1.3 dynamic_slice.6
  1.9 1.3 pad_dynamic-slice_fusion.taps
  3.3 0.9 copy.19
  4.1 0.0 copy-start
  4.2 0.1 slice_negate_fusion.2
  4.3 0.5 fusion.7
  4.8 0.0 copy-done.3
  4.8 0.1 reshape.87
  4.8 0.2 fusion.8
  5.1 0.0 copy-done
  5.1 0.4 reshape.86
  5.5 0.1 slice.17
  5.6 0.3 slice_negate_fusion
  5.9 0.3 fusion.3
  6.2 0.0 copy-start.4
  6.2 0.0 copy-start.1
  6.2 0.1 slice.16
  6.3 0.1 pad.21.clone
  6.4 0.8 maximum_bitcast_fusion.qw
  7.3 0.8 maximum_bitcast_fusion.1.qn
  8.1 0.0 copy-start.2
  8.1 0.1 pad.26.clone
  8.2 0.0 copy-done.4
  8.2 0.7 maximum_maximum_fusion.lat_in
  8.9 0.0 copy-done.1
  8.9 0.1 copy.24
  9.1 1.0 copy.28.kun
  10.1 0.0 copy-done.2
  10.1 0.1 copy.26
  10.3 1.0 copy.29.vun
  11.3 151.7 %layer.1 = bf16[96,2048]{1,0:T(8,128)(2,1)} custom-call(bf16[192,640]{1,0:T(8,128)(2,1)} %maximum_maximum_fusion.lat_in, bf16[4,192,256]{2,1,0:T(8,128)(2,1)} %maximum_bitcast_fusion.qw, bf16[4,192,128]{2,1,0:T(8,128)(2,1)} %maximum_bitcast_fusion.1.qn, f32[1,2048]{1,0:T(1,128)} %bitcast.14, f32[3,768]{1,0:T(4,128)} %pad_dynamic-slice_fusion.taps, ...), custom_call_target="tpu_custom_call" | custom-call | tf_op jit(solution)/shard_map/layer/pallas_call | solution.py:620
  163.0 1.8 %copy.41 = bf16[96,2048]{1,0:T(8,128)(2,1)} copy(bf16[96,2048]{1,0:T(8,128)(2,1)} %layer.1) | data formatting | bytes 786432
  (11 shorter events, 0.2 us)
Async XLA Ops:
  0.0 4.8 %copy-start.3 = (bf16[192,512]{1,0:T(8,128)(2,1)S(1)}, bf16[192,512]{1,0:T(8,128)(2,1)}, u32[]{:S(2)}) copy-start(bf16[192,512]{1,0:T(8,128)(2,1)} %param.21) | copy-start | bytes 589828
  4.1 1.0 copy-start
  6.2 2.0 %copy-start.4 = (bf16[192,512]{1,0:T(8,128)(2,1)S(1)}, bf16[192,512]{1,0:T(8,128)(2,1)}, u32[]{:S(2)}) copy-start(bf16[192,512]{1,0:T(8,128)(2,1)} %param.18) | copy-start | bytes 589828
  6.2 2.7 %copy-start.1 = (bf16[512,256]{1,0:T(8,128)(2,1)S(1)}, bf16[512,256]{1,0:T(8,128)(2,1)}, u32[]{:S(2)}) copy-start(bf16[512,256]{1,0:T(8,128)(2,1)} %param.24) | copy-start | bytes 786436
  8.1 2.0 %copy-start.2 = (bf16[512,256]{1,0:T(8,128)(2,1)S(1)}, bf16[512,256]{1,0:T(8,128)(2,1)}, u32[]{:S(2)}) copy-start(bf16[512,256]{1,0:T(8,128)(2,1)} %param.25) | copy-start | bytes 786436
where the time goes:
time: 165 us
  Pallas kernels  152 us (92%)
  local copies, waits for them, and re-layouts  8.6 us (5%)
  other arithmetic  3.65 us (2%)
    pallas_call x1, Pallas kernels, layer(): pl.pallas_call(functools.partial(layer_kernel, n), out_shape=jax.ShapeDty...  152 us

commit v1 on v0

v1 whole, which is shorter than its diff:
```python
import functools
import math

import jax
import jax.numpy as jnp
from jax import lax
from jax.experimental import pallas as pl
from jax.experimental.pallas import tpu as pltpu
from jax.sharding import PartitionSpec as P

NOPE_W = 128
NOPE_N = 64
LANES = 128
MESH = pl.DeviceIdType.MESH
BF = jnp.bfloat16
F32 = jnp.float32

rope_base = 10000.0
norm_eps = 1e-06


def cut_points(tiles, parts):
    plain = [k * tiles // parts for k in range(parts + 1)]
    even = [
        k * tiles // parts if 2 * k <= parts else tiles - (parts - k) * tiles // parts
        for k in range(parts + 1)
    ]

    def widest(cuts):
        return max(b - a for a, b in zip(cuts, cuts[1:]))

    return even if widest(even) <= widest(plain) else plain


def dot(a, b):
    return jnp.dot(a, b, preferred_element_type=F32)


def dot_t(a, b):
    return lax.dot_general(a, b, (((1,), (1,)), ((), ())), preferred_element_type=F32)


def layer_kernel(
    n,
    latent, rope, query_w, query_n, trig, gain,
    x_in, kuw, kun, vuw, vun, ow, on, conv, gate, value, down,
    out,
    lat, kuw_v, kun_v, vuw_v, vun_v, ow_v, xin_v,
    taps, qw, qn, kw, kn, vw, vn, att, hpb, hrecv, mid,
    wg, wv, wd, xs, gp, vp, edge, halo, hid, pb, xr, zin,
    loc,
    lz_s, lz_r, lx_s, lx_r, lc_s, lc_r, lo_s, lo_r,
    wz_s, wz_r, wy_s, wy_r, wc_s, wc_r, wl,
    hx_s, hx_r, azr_s, azl_s, az_r, ax_s, ax_r, e_s, e_r,
    rx_s, rx_r, rz_s, rz_r,
):
    G, S, T = n["G"], n["S"], n["T"]
    Z = S // 2
    R = latent.shape[0]
    B = R // T
    LW = kuw.shape[0]
    D = xs.shape[3]
    HW, HN = qw.shape[0], qn.shape[0]
    WMAX = wg.shape[3]
    depth = gate.shape[0]
    cuts = cut_points(gate.shape[1] // LANES, Z)
    widths = [(b - a) * LANES for a, b in zip(cuts, cuts[1:])]
    g, s, t = lax.axis_index("grp"), lax.axis_index("sp"), lax.axis_index("tp")
    z, c = s // 2, s % 2

    def zdev(zz):
        return (g, 2 * zz + c, t)

    def xdev(tt):
        return (g, s, tt)

    sib = (g, 2 * z + 1 - c, t)
    xpart = [(t + d) % T for d in range(1, T)]
    if n["share"]:
        pb = xs

    def slot(sender, receiver):
        return (sender - receiver + T) % T - 1

    ypart = [(g + d) % G for d in range(1, G)]

    def rcopy(src, dst, ss, rs, dev):
        return pltpu.make_async_remote_copy(
            src_ref=src, dst_ref=dst, send_sem=ss, recv_sem=rs, device_id=dev, device_id_type=MESH
        )

    def got(ref, rs):
        rcopy(ref, ref, rs, rs, sib).wait_recv()

    def sent(ref, ss):
        rcopy(ref, ref, ss, ss, sib).wait_send()

    def rows(part):
        return pl.ds(pl.multiple_of(part * B, B), B)

    def by_lane(first, second, width):
        lane = lax.broadcasted_iota(jnp.int32, (R, LANES), 1)
        return jnp.where(lane < width, first, second)

    def turn(entries):
        turned = by_lane(-pltpu.roll(entries, LANES - 32, 1), pltpu.roll(entries, 32, 1), 32)
        return entries * trig[0] + turned * trig[1]

    local = [
        pltpu.make_async_copy(kuw, kuw_v, loc.at[0]),
        pltpu.make_async_copy(kun, kun_v, loc.at[1]),
        pltpu.make_async_copy(vuw, vuw_v, loc.at[2]),
        pltpu.make_async_copy(vun, vun_v, loc.at[3]),
        pltpu.make_async_copy(x_in, xin_v, loc.at[4]),
        pltpu.make_async_copy(ow, ow_v.at[pl.ds(0, HW * LANES)], loc.at[5]),
        pltpu.make_async_copy(on, ow_v.at[pl.ds(HW * LANES, HN * NOPE_N)], loc.at[6]),
    ]
    for cp in local:
        cp.start()
    lat[s, :, pl.ds(0, LW)] = latent[...]
    entries = jnp.concatenate([rope[...].astype(F32), jnp.zeros((R, LANES - rope.shape[1]), F32)], 1)
    lat[s, :, pl.ds(LW, LANES)] = turn(entries).astype(BF)

    bar = pltpu.get_barrier_semaphore()
    for zz in range(Z):
        @pl.when(zz != z)
        def _():
            pl.semaphore_signal(bar, inc=1, device_id=zdev(zz), device_id_type=MESH)
    for tt in xpart:
        pl.semaphore_signal(bar, inc=1, device_id=xdev(tt), device_id_type=MESH)
    for gg in ypart:
        pl.semaphore_signal(bar, inc=1, device_id=(gg, s, t), device_id_type=MESH)
    pl.semaphore_signal(bar, inc=1, device_id=sib, device_id_type=MESH)
    pl.semaphore_wait(bar, Z + T + G - 2)

    for zz in range(Z):
        @pl.when(zz != z)
        def _():
            part = lat.at[s, rows(t)]
            rcopy(part, part, lz_s.at[zz], lz_r.at[z], zdev(zz)).start()
    rcopy(lat.at[s], lat.at[s], lo_s, lo_r, sib).start()

    mats = ((gate, wg), (value, wv), (down, wd))
    hd = depth // G

    def piece(ai, zz, cc, gg, w):
        if ai < 2:
            return mats[ai][1].at[zz, cc, pl.ds(pl.multiple_of(gg * hd, hd), hd), pl.ds(0, w)]
        wh = w // G
        return wd.at[zz, cc, pl.ds(pl.multiple_of(gg * wh, wh), wh)]

    def slab(ai, cc, w):
        if ai < 2:
            return mats[ai][1].at[:, cc, :, pl.ds(0, w)]
        return wd.at[:, cc, pl.ds(0, w)]

    def own_copy(ai, zz):
        w, lo = widths[zz], cuts[zz] * LANES
        if ai < 2:
            return pltpu.make_async_copy(
                mats[ai][0].at[:, pl.ds(lo, w)], mats[ai][1].at[zz, c, :, pl.ds(0, w)], wl.at[ai]
            )
        return pltpu.make_async_copy(down.at[pl.ds(lo, w)], wd.at[zz, c, pl.ds(0, w)], wl.at[ai])

    def tap_copy(zz):
        w = widths[zz]
        return pltpu.make_async_copy(
            conv.at[:, pl.ds(cuts[zz] * LANES, w)], taps.at[:, pl.ds(0, w)], loc.at[7]
        )

    def hbm_piece(ai, zz):
        w, lo = widths[zz], cuts[zz] * LANES
        if ai < 2:
            return mats[ai][0].at[pl.ds(pl.multiple_of(g * hd, hd), hd), pl.ds(lo, w)]
        wh = w // G
        return down.at[pl.ds(pl.multiple_of(lo + g * wh, math.gcd(lo, wh) if lo else wh), wh)]

    def spread(ai):
        for zz in range(Z):
            if widths[zz]:
                @pl.when(zz != z)
                def _():
                    rcopy(
                        hbm_piece(ai, zz), piece(ai, z, c, g, widths[zz]),
                        wz_s.at[ai, zz], wz_r.at[ai, z], zdev(zz),
                    ).start()

                @pl.when(zz == z)
                def _():
                    own_copy(ai, zz).start()

    def by_width(body):
        for w in sorted(set(widths)):
            mine = functools.reduce(
                jnp.logical_or, [z == k for k in range(Z) if widths[k] == w]
            )

            @pl.when(mine)
            def _():
                body(w)

    def relay_y(ai):
        def body(w):
            if not w:
                return
            for zz in range(Z):
                @pl.when(zz != z)
                def _():
                    part = piece(ai, zz, c, g, w)
                    got(part, wz_r.at[ai, zz])
                    for gg in ypart:
                        rcopy(part, part, wy_s.at[ai, zz, gg], wy_r.at[ai, zz, g], (gg, s, t)).start()
        by_width(body)

    def relay_core(ai):
        def body(w):
            if not w:
                return
            for zz in range(Z):
                if widths[zz] == w:
                    @pl.when(zz == z)
                    def _():
                        own_copy(ai, zz).wait()
            for zz in range(Z):
                @pl.when(zz != z)
                def _():
                    for gg in ypart:
                        got(piece(ai, zz, c, gg, w), wy_r.at[ai, zz, gg])
            rcopy(slab(ai, c, w), slab(ai, c, w), wc_s.at[ai], wc_r.at[ai], sib).start()
        by_width(body)

    def arrive(ai):
        def body(w):
            if w:
                got(slab(ai, 1 - c, w), wc_r.at[ai])
        by_width(body)

    def spread_sent(ai):
        for zz in range(Z):
            if widths[zz]:
                @pl.when(zz != z)
                def _():
                    sent(hbm_piece(ai, zz), wz_s.at[ai, zz])

        def body(w):
            if not w:
                return
            for zz in range(Z):
                @pl.when(zz != z)
                def _():
                    for gg in ypart:
                        sent(piece(ai, zz, c, g, w), wy_s.at[ai, zz, gg])
            sent(slab(ai, c, w), wc_s.at[ai])
        by_width(body)

    spread(0)
    spread(1)

    for zz in range(Z):
        if widths[zz]:
            @pl.when(zz == z)
            def _():
                tap_copy(zz).start()

    def clear(w):
        if w < WMAX:
            gap = WMAX - w
            for ref in (wg, wv):
                ref[:, :, :, pl.ds(w, gap)] = jnp.zeros((Z, 2, depth, gap), BF)
            wd[:, :, pl.ds(w, gap), :] = jnp.zeros((Z, 2, gap, wd.shape[3]), BF)
            taps[:, pl.ds(w, gap)] = jnp.zeros((taps.shape[0], gap), F32)
    by_width(clear)

    for h in range(0, HW, 2):
        one, two, three = (
            query_w[:, pl.ds((3 * (h // 2) + i) * LANES, LANES)].astype(F32) for i in range(3)
        )
        two_r, three_r = pltpu.roll(two, 64, 1), pltpu.roll(three, 64, 1)
        qw[h, :, pl.ds(0, LANES)] = one.astype(BF)
        qw[h, :, pl.ds(LANES, LANES)] = turn(two).astype(BF)
        qw[h + 1, :, pl.ds(0, LANES)] = by_lane(two_r, three_r, 64).astype(BF)
        qw[h + 1, :, pl.ds(LANES, LANES)] = turn(three_r).astype(BF)
    for h in range(HN):
        entries = pltpu.roll(query_n[:, pl.ds(h * LANES, LANES)].astype(F32), 64, 1)
        qn[h] = by_lane(turn(entries), entries, 64).astype(BF)
    for cp in local[:4]:
        cp.wait()

    def expand(i):
        at = pl.ds(pl.multiple_of(i * R, R), R)
        low = lat[i, :, pl.ds(0, LW)]
        turned = lat[i, :, pl.ds(LW, LANES)]
        key = dot(low, kuw_v[...]).astype(BF)
        val = dot(low, vuw_v[...]).astype(BF)
        for h in range(HW):
            kw[h, at, pl.ds(0, LANES)] = key[:, h * LANES : (h + 1) * LANES]
            kw[h, at, pl.ds(LANES, LANES)] = turned
            vw[h, at, :] = val[:, h * LANES : (h + 1) * LANES]
        key = dot(low, kun_v[...]).astype(BF).astype(F32)
        val = dot(low, vun_v[...]).astype(BF)
        turned = turned.astype(F32)
        for h in range(0, HN, 2):
            pair = key[:, h * NOPE_N : h * NOPE_N + LANES]
            kn[h, at, :] = by_lane(turned, pltpu.roll(pair, 64, 1), 64).astype(BF)
            kn[h + 1, at, :] = by_lane(turned, pair, 64).astype(BF)
            vn[h // 2, at, :] = val[:, h * NOPE_N : h * NOPE_N + LANES]

    for zz in range(Z):
        @pl.when(zz != z)
        def _():
            part = lat.at[2 * zz + c, rows(t)]
            got(part, lz_r.at[zz])
            for tt in xpart:
                rcopy(part, part, lx_s.at[zz, tt], lx_r.at[zz, t], xdev(tt)).start()
            rcopy(part, part, lc_s.at[zz, t], lc_r.at[zz, t], sib).start()
    expand(s)

    def mine(zz, carry):
        @pl.when(zz != z)
        def _():
            for tt in xpart:
                part = lat.at[2 * zz + c, rows(tt)]
                got(part, lx_r.at[zz, tt])
                rcopy(part, part, lc_s.at[zz, tt], lc_r.at[zz, tt], sib).start()
            expand(2 * zz + c)
        return carry

    lax.fori_loop(0, Z, mine, 0)
    got(lat.at[2 * z + 1 - c], lo_r)
    expand(2 * z + 1 - c)

    def theirs(zz, carry):
        @pl.when(zz != z)
        def _():
            for tt in range(T):
                got(lat.at[2 * zz + 1 - c, rows(tt)], lc_r.at[zz, tt])
            expand(2 * zz + 1 - c)
        return carry

    lax.fori_loop(0, Z, theirs, 0)

    def attend(q, k, v, scale):
        score = dot_t(q, k) * (scale * math.log2(math.e))
        prob = jnp.exp2(score - jnp.max(score, axis=-1, keepdims=True))
        total = jnp.sum(prob, axis=-1, keepdims=True)
        return dot(prob.astype(BF), v) / total

    def wide(h, carry):
        at = pl.ds(pl.multiple_of(h * LANES, LANES), LANES)
        att[:, at] = attend(qw[h], kw[h], vw[h], n["scale_w"]).astype(BF)
        return carry

    def narrow(p, carry):
        at = pl.ds(pl.multiple_of((HW + p) * LANES, LANES), LANES)
        first = attend(qn[2 * p], kn[2 * p], vn[p], n["scale_n"])
        second = attend(qn[2 * p + 1], kn[2 * p + 1], vn[p], n["scale_n"])
        att[:, at] = by_lane(first, second, 64).astype(BF)
        return carry

    lax.fori_loop(0, HW, wide, 0)
    relay_y(0)
    lax.fori_loop(0, HN // 2, narrow, 0)

    for cp in local[4:]:
        cp.wait()
    NB = n["NB"]
    cw = D // NB
    for j in range(NB):
        cols = pl.ds(j * cw, cw)
        hpb[:, cols] = dot(att[...], ow_v[:, cols]).astype(BF)
        for tt in xpart:
            rcopy(
                hpb.at[rows(tt), cols], hrecv.at[slot(t, tt), :, cols], hx_s.at[tt, j], hx_r.at[t, j], xdev(tt)
            ).start()
    for j in range(NB):
        cols = pl.ds(j * cw, cw)
        part = hpb[rows(t), cols].astype(F32)
        for tt in xpart:
            came = hrecv.at[slot(tt, t), :, cols]
            got(came, hx_r.at[tt, j])
            part = part + came[...].astype(F32)
        mid[:, cols] = (xin_v[:, cols].astype(F32) + part).astype(BF).astype(F32)
    full = mid[...]
    power = jnp.mean(full * full, axis=-1, keepdims=True)
    xs[z, t] = (full * lax.rsqrt(power + norm_eps) * gain[...]).astype(BF)

    U = n["U"]
    sub = B // U

    def strip(zi, tt, u):
        return xs.at[zi, tt, pl.ds(u * sub, sub)]

    def forward(zi, u):
        blk = strip(zi, t, u)

        @pl.when((zi <= z) & (z < Z - 1))
        def _():
            rcopy(blk, blk, azr_s.at[zi, u], az_r.at[zi, u], zdev(z + 1)).start()

        @pl.when((zi >= z) & (z > 0))
        def _():
            rcopy(blk, blk, azl_s.at[zi, u], az_r.at[zi, u], zdev(z - 1)).start()
        for tt in xpart:
            rcopy(blk, blk, ax_s.at[zi, tt, u], ax_r.at[zi, t, u], xdev(tt)).start()

    def rows_sent():
        for zz in range(Z):
            for u in range(U):
                @pl.when((zz <= z) & (z < Z - 1))
                def _():
                    sent(strip(zz, t, u), azr_s.at[zz, u])

                @pl.when((zz >= z) & (z > 0))
                def _():
                    sent(strip(zz, t, u), azl_s.at[zz, u])
                for tt in xpart:
                    sent(strip(zz, t, u), ax_s.at[zz, tt, u])

    near = jnp.minimum(z, Z - 1 - z)
    outward = jnp.where(z < Z - 1 - z, 1, -1)

    def order(i):
        sign = jnp.where(i % 2 == 1, 1, -1)
        return jnp.where(i <= 2 * near, z + sign * ((i + 1) // 2), z + outward * (i - near))

    def relay_rows(i):
        nxt = order(i)
        for u in range(U):
            got(strip(nxt, t, u), az_r.at[nxt, u])
            forward(nxt, u)

    for u in range(U):
        forward(z, u)
    relay_y(1)
    if Z > 1:
        relay_rows(1)
    spread(2)
    relay_core(0)
    arrive(0)
    relay_core(1)
    arrive(1)

    NC = WMAX // n["NW"]

    def project(i, carry):
        zi = order(i)

        for tt in xpart:
            for u in range(U):
                got(strip(zi, tt, u), ax_r.at[zi, tt, u])
        block = xs[zi].reshape(R, D)
        for j in range(n["NW"]):
            cols = pl.ds(j * NC, NC)
            pre = dot(block, wg[:, :, :, cols].reshape(D, NC)).astype(BF)
            gp[zi, :, cols] = pre
            edge[zi, pl.ds(0, 8), cols] = pre[:8].astype(F32)
            edge[zi, pl.ds(8, 8), cols] = pre[R - 8 :].astype(F32)
        for j in range(n["NW"]):
            cols = pl.ds(j * NC, NC)
            vp[zi, :, cols] = dot(block, wv[:, :, :, cols].reshape(D, NC)).astype(vp.dtype)

        @pl.when(i + 2 < Z)
        def _():
            relay_rows(i + 2)

        @pl.when(i == max(0, Z - 3))
        def _():
            relay_y(2)
        return carry

    lax.fori_loop(0, Z, project, 0)
    rcopy(edge, halo, e_s, e_r, sib).start()
    relay_core(2)
    arrive(2)
    got(halo, e_r)
    for zz in range(Z):
        if widths[zz]:
            @pl.when(zz == z)
            def _():
                tap_copy(zz).wait()
    if n["share"]:
        rows_sent()

    place = lax.broadcasted_iota(jnp.int32, (R, NC), 0)
    OW = wd.shape[3]

    J = 2
    SJ = S // J
    DJ = D // J

    def summed(zi, j):
        cols = pl.ds(j * DJ, DJ)
        total = pb[zi, t, :, cols].astype(F32)
        for tt in xpart:
            part = xr.at[zi, slot(tt, t), :, cols]
            got(part, rx_r.at[zi, tt, j])
            total = total + part[...].astype(F32)
        return total

    def add_up(zi, j):
        cols = pl.ds(j * DJ, DJ)
        total = summed(zi, j)
        inner = ((zi > z) & (z > 0)) | ((zi < z) & (z < Z - 1))
        mine = pb.at[zi, t, :, cols]

        @pl.when(inner)
        def _():
            got(zin.at[zi, :, cols], rz_r.at[zi, j])
            mine[...] = (total + zin[zi, :, cols].astype(F32)).astype(BF)

        @pl.when(jnp.logical_not(inner))
        def _():
            mine[...] = total.astype(BF)

        @pl.when(zi > z)
        def _():
            rcopy(mine, zin.at[zi, :, cols], rz_s.at[zi, j], rz_r.at[zi, j], zdev(z + 1)).start()

        @pl.when(zi < z)
        def _():
            into = jnp.where(zi == z - 1, Z, zi)
            rcopy(mine, zin.at[into, :, cols], rz_s.at[zi, j], rz_r.at[into, j], zdev(z - 1)).start()

    def mix(k, carry):
        zi = order(Z - 1 - k)
        above, below = zi - 1 + c, zi + c
        has_above = jnp.where(above >= 0, 1.0, 0.0)
        has_below = jnp.where(below < Z, 1.0, 0.0)
        above, below = jnp.maximum(above, 0), jnp.minimum(below, Z - 1)
        for j in range(n["NW"]):
            cols = pl.ds(j * NC, NC)
            pre = gp[zi, :, cols].astype(F32)
            prev = halo[above, pl.ds(8, 8), cols][7:8] * has_above
            post = halo[below, pl.ds(0, 8), cols][0:1] * has_below
            up = jnp.where(place == 0, prev, pltpu.roll(pre, 1, 0))
            dn = jnp.where(place == R - 1, post, pltpu.roll(pre, R - 1, 0))
            conv = taps[0:1, cols] * up + taps[1:2, cols] * pre + taps[2:3, cols] * dn
            hid[:, cols] = (conv / (1.0 + jnp.exp(-conv)) * vp[zi, :, cols].astype(F32)).astype(BF)
        for j in range(J):
            for b in range(j * SJ, j * SJ + SJ):
                part = dot(hid[...], wd[b // 2, b % 2]).astype(BF)
                pb[zi, :, :, pl.ds(b * OW, OW)] = part.reshape(T, B, OW)
            cols = pl.ds(j * DJ, DJ)
            for tt in xpart:
                rcopy(
                    pb.at[zi, tt, :, cols], xr.at[zi, slot(t, tt), :, cols],
                    rx_s.at[zi, tt, j], rx_r.at[zi, t, j], xdev(tt),
                ).start()
        return carry

    lax.fori_loop(0, Z, mix, 0)

    def pass_on(k, carry):
        zi = order(Z - 1 - k)
        for j in range(J):
            add_up(zi, j)
        return carry

    lax.fori_loop(0, Z - 1, pass_on, 0)
    for j in range(J):
        cols = pl.ds(j * DJ, DJ)
        mid[:, cols] = mid[:, cols] + summed(z, j)

        @pl.when(z > 0)
        def _():
            got(zin.at[z, :, cols], rz_r.at[z, j])
            mid[:, cols] = mid[:, cols] + zin[z, :, cols].astype(F32)

        @pl.when(z < Z - 1)
        def _():
            got(zin.at[Z, :, cols], rz_r.at[Z, j])
            mid[:, cols] = mid[:, cols] + zin[Z, :, cols].astype(F32)
    out[...] = mid[...].astype(BF)

    sent(lat.at[s], lo_s)
    sent(edge, e_s)
    for ai in range(3):
        spread_sent(ai)
    for tt in xpart:
        for j in range(NB):
            sent(hpb.at[rows(tt), pl.ds(j * cw, cw)], hx_s.at[tt, j])
    for zz in range(Z):
        @pl.when(zz != z)
        def _():
            part = lat.at[2 * zz + c, rows(t)]
            sent(part, lz_s.at[zz])
            for tt in xpart:
                sent(part, lx_s.at[zz, tt])
            for tt in range(T):
                sent(part, lc_s.at[zz, tt])
            for j in range(J):
                sent(pb.at[zz, t, :, pl.ds(j * DJ, DJ)], rz_s.at[zz, j])
        for tt in xpart:
            for j in range(J):
                sent(pb.at[zz, tt, :, pl.ds(j * DJ, DJ)], rx_s.at[zz, tt, j])
    if not n["share"]:
        rows_sent()


def rope_tables(row_start, row_total, span_width):
    places = (row_start + jnp.arange(row_total, dtype=jnp.int32)).astype(F32)
    frequency = jnp.power(
        rope_base, -jnp.arange(0, span_width, 2, dtype=jnp.int32).astype(F32) / span_width
    )
    angles = places[:, None] * jnp.tile(frequency, 2 * LANES // span_width)[None, :]
    valid = jnp.arange(LANES) < span_width
    return jnp.where(valid, jnp.stack([jnp.cos(angles), jnp.sin(angles)]), 0.0)


def layer(
    layer_input,
    latent,
    rope_key,
    query_wide,
    query_narrow,
    key_up_wide,
    value_up_wide,
    key_up_narrow,
    value_up_narrow,
    out_wide,
    out_narrow,
    norm_gain,
    gate_weight,
    value_weight,
    conv_weight,
    down_weight,
):
    G, S, T = lax.axis_size("grp"), lax.axis_size("sp"), lax.axis_size("tp")
    Z = S // 2
    R, LW = latent.shape
    rot = rope_key.shape[1]
    D = layer_input.shape[1]
    B = R // T
    HW = key_up_wide.shape[1] // NOPE_W
    HN = key_up_narrow.shape[1] // NOPE_N
    trig = rope_tables(lax.axis_index("sp") * R, R, rot)
    tiles = gate_weight.shape[1] // LANES
    cuts = cut_points(tiles, Z)
    wmax = max(b - a for a, b in zip(cuts, cuts[1:])) * LANES
    keys = S * R
    depth, ow = gate_weight.shape[0], down_weight.shape[1]
    U = 2 if B % 32 == 0 else 1
    share = Z * T * B * D * 2 > 8 << 20
    n = dict(
        share=share,
        U=U,
        G=G,
        S=S,
        T=T,
        NB=4,
        NW=max(1, wmax // 256),
        scale_w=1.0 / math.sqrt(NOPE_W + rot),
        scale_n=1.0 / math.sqrt(NOPE_N + rot),
    )
    vmem = pl.BlockSpec(memory_space=pltpu.VMEM)
    hbm = pl.BlockSpec(memory_space=pl.ANY)

    def V(*shape, dtype=BF):
        return pltpu.VMEM(shape, dtype)

    def sem(*shape):
        return pltpu.SemaphoreType.DMA(shape)

    one = pltpu.SemaphoreType.DMA
    scratch = [
        V(S, R, LW + LANES),
        V(*key_up_wide.shape), V(*key_up_narrow.shape),
        V(*value_up_wide.shape), V(*value_up_narrow.shape),
        V(HW * LANES + HN * NOPE_N, D), V(B, D), V(conv_weight.shape[0], wmax, dtype=F32),
        V(HW, R, 2 * LANES), V(HN, R, LANES),
        V(HW, keys, 2 * LANES), V(HN, keys, LANES), V(HW, keys, LANES), V(HN // 2, keys, LANES),
        V(R, HW * LANES + HN * NOPE_N), V(R, D), V(T - 1, B, D), V(B, D, dtype=F32),
        V(Z, 2, depth, wmax), V(Z, 2, depth, wmax), V(Z, 2, wmax, ow),
        V(Z, T, B, D), V(Z, R, wmax), V(Z, R, wmax, dtype=BF if share else F32),
        V(Z, 16, wmax, dtype=F32), V(Z, 16, wmax, dtype=F32), V(R, wmax),
        V(8, LANES) if share else V(Z, T, B, D), V(Z, T - 1, B, D), V(Z + 1, B, D),
        sem(8),
        sem(Z), sem(Z), sem(Z, T), sem(Z, T), sem(Z, T), sem(Z, T), one, one,
        sem(3, Z), sem(3, Z), sem(3, Z, G), sem(3, Z, G), sem(3), sem(3), sem(3),
        sem(T, 4), sem(T, 4), sem(Z, U), sem(Z, U), sem(Z, U), sem(Z, T, U), sem(Z, T, U), one, one,
        sem(Z, T, 2), sem(Z, T, 2), sem(Z, 2), sem(Z + 1, 2),
    ]
    return pl.pallas_call(
        functools.partial(layer_kernel, n),
        out_shape=jax.ShapeDtypeStruct((B, D), BF),
        in_specs=[vmem] * 6 + [hbm] * 11,
        out_specs=vmem,
        scratch_shapes=scratch,
        compiler_params=pltpu.CompilerParams(
            collective_id=0, has_side_effects=True, vmem_limit_bytes=67043328
        ),
        name="layer",
    )(
        latent, rope_key, query_wide, query_narrow, trig, norm_gain.reshape(1, D),
        layer_input, key_up_wide, key_up_narrow, value_up_wide, value_up_narrow,
        out_wide, out_narrow, conv_weight, gate_weight, value_weight, down_weight,
    )


def solution(mesh):
    in_specs = (
        P(("grp", "sp", "tp"), None),
        P(("grp", "sp"), None),
        P(("grp", "sp"), None),
        P(("grp", "sp"), "tp"),
        P(("grp", "sp"), "tp"),
        P(None, "tp"),
        P(None, "tp"),
        P(None, "tp"),
        P(None, "tp"),
        P("tp", None),
        P("tp", None),
        P(),
        P("sp", "tp"),
        P("sp", "tp"),
        P(None, "tp"),
        P("tp", "sp"),
    )
    out_specs = P(("grp", "sp", "tp"), None)
    return jax.shard_map(
        layer, mesh=mesh, in_specs=in_specs, out_specs=out_specs, check_vma=False
    )
```

time: 165 us -> 147 us (0.89)
  the two profiles are of different devices: /device:TPU:16 before, /device:TPU:25 now
where the time goes in v1:
time: 147 us
  Pallas kernels  142 us (97%)
  local copies, waits for them, and re-layouts  3.34 us (2%)
    pallas_call x1, Pallas kernels, layer(): pl.pallas_call(functools.partial(layer_kernel, n), out_shape=jax.ShapeDty...  142 us
    unnamed x2, local copies, waits for them, and re-layouts  3.25 us

profile of v1, /device:TPU:25, one launch (start us, length us, event | category | flops | bytes accessed | tf_op | source)
XLA Modules:
  0.0 146.9 jit_solution(13243232943901849983)
XLA Ops:
  0.0 0.1 mul.43
  0.1 1.5 %copy.17.rope = bf16[192,64]{1,0:T(8,128)(2,1)} copy(bf16[192,64]{0,1:T(8,128)(2,1)} %param.18) | data formatting | bytes 49152 | tf_op args[2]
  1.6 0.4 multiply_cosine_fusion
  2.0 0.7 maximum_select_fusion.trig
  2.7 142.4 %layer.1 = bf16[96,2048]{1,0:T(8,128)(2,1)} custom-call(bf16[192,512]{1,0:T(8,128)(2,1)} %latent.1, bf16[192,64]{1,0:T(8,128)(2,1)} %copy.17.rope, bf16[192,768]{1,0:T(8,128)(2,1)} %query_w.1, bf16[192,512]{1,0:T(8,128)(2,1)} %query_n.1, f32[2,192,128]{2,1,0:T(8,128)} %maximum_select_fusion.trig, f32[1,2048]{1,0:T(1,128)} %bitcast.1, bf16[96,2048]{1,0:T(8,128)(2,1)} %x_in.1, ...), custom_call_target="tpu_custom_call" | custom-call | tf_op jit(solution)/shard_map/layer/pallas_call | solution.py:683
  145.1 1.8 %copy.19 = bf16[96,2048]{1,0:T(8,128)(2,1)} copy(bf16[96,2048]{1,0:T(8,128)(2,1)} %layer.1) | data formatting | bytes 786432
  (4 shorter events, 0.0 us)

commit v2 on v1

--- a/solution.py
+++ b/solution.py
@@ -49,7 +49,7 @@
     taps, qw, qn, kw, kn, vw, vn, att, hpb, hrecv, mid,
     wg, wv, wd, xs, gp, vp, edge, halo, hid, pb, xr, zin,
     loc,
-    lz_s, lz_r, lx_s, lx_r, lc_s, lc_r, lo_s, lo_r,
+    lzr_s, lzl_s, lz_r, lx_s, lx_r, lc_s, lc_r, lo_s, lo_r,
     wz_s, wz_r, wy_s, wy_r, wc_s, wc_r, wl,
     hx_s, hx_r, azr_s, azl_s, az_r, ax_s, ax_r, e_s, e_r,
     rx_s, rx_r, rz_s, rz_r,
@@ -118,7 +118,12 @@
     for cp in local:
         cp.start()
     lat[s, :, pl.ds(0, LW)] = latent[...]
-    entries = jnp.concatenate([rope[...].astype(F32), jnp.zeros((R, LANES - rope.shape[1]), F32)], 1)
+    rot = rope.shape[0]
+    wide_rows = -(-R // LANES) * LANES
+    entries = jnp.concatenate([rope[...].astype(F32), jnp.zeros((LANES - rot, R), F32)], 0)
+    if wide_rows > R:
+        entries = jnp.concatenate([entries, jnp.zeros((LANES, wide_rows - R), F32)], 1)
+    entries = entries.T[:R]
     lat[s, :, pl.ds(LW, LANES)] = turn(entries).astype(BF)
 
     bar = pltpu.get_barrier_semaphore()
@@ -133,11 +138,25 @@
     pl.semaphore_signal(bar, inc=1, device_id=sib, device_id_type=MESH)
     pl.semaphore_wait(bar, Z + T + G - 2)
 
-    for zz in range(Z):
-        @pl.when(zz != z)
-        def _():
-            part = lat.at[s, rows(t)]
-            rcopy(part, part, lz_s.at[zz], lz_r.at[z], zdev(zz)).start()
+    near = jnp.minimum(z, Z - 1 - z)
+    outward = jnp.where(z < Z - 1 - z, 1, -1)
+
+    def order(i):
+        sign = jnp.where(i % 2 == 1, 1, -1)
+        return jnp.where(i <= 2 * near, z + sign * ((i + 1) // 2), z + outward * (i - near))
+
+    def pass_latents(zi):
+        part = lat.at[2 * zi + c, rows(t)]
+
+        @pl.when((zi <= z) & (z < Z - 1))
+        def _():
+            rcopy(part, part, lzr_s.at[zi], lz_r.at[zi], zdev(z + 1)).start()
+
+        @pl.when((zi >= z) & (z > 0))
+        def _():
+            rcopy(part, part, lzl_s.at[zi], lz_r.at[zi], zdev(z - 1)).start()
+
+    pass_latents(z)
     rcopy(lat.at[s], lat.at[s], lo_s, lo_r, sib).start()
 
     mats = ((gate, wg), (value, wv), (down, wd))
@@ -253,8 +272,6 @@
             sent(slab(ai, c, w), wc_s.at[ai])
         by_width(body)
 
-    spread(0)
-    spread(1)
 
     for zz in range(Z):
         if widths[zz]:
@@ -305,14 +322,16 @@
             kn[h + 1, at, :] = by_lane(turned, pair, 64).astype(BF)
             vn[h // 2, at, :] = val[:, h * NOPE_N : h * NOPE_N + LANES]
 
-    for zz in range(Z):
-        @pl.when(zz != z)
-        def _():
-            part = lat.at[2 * zz + c, rows(t)]
-            got(part, lz_r.at[zz])
-            for tt in xpart:
-                rcopy(part, part, lx_s.at[zz, tt], lx_r.at[zz, t], xdev(tt)).start()
-            rcopy(part, part, lc_s.at[zz, t], lc_r.at[zz, t], sib).start()
+    for i in range(1, Z):
+        zi = order(i)
+        part = lat.at[2 * zi + c, rows(t)]
+        got(part, lz_r.at[zi])
+        pass_latents(zi)
+        for tt in xpart:
+            rcopy(part, part, lx_s.at[zi, tt], lx_r.at[zi, t], xdev(tt)).start()
+        rcopy(part, part, lc_s.at[zi, t], lc_r.at[zi, t], sib).start()
+    spread(0)
+    spread(1)
     expand(s)
 
     def mine(zz, carry):
@@ -415,13 +434,6 @@
                     sent(strip(zz, t, u), azl_s.at[zz, u])
                 for tt in xpart:
                     sent(strip(zz, t, u), ax_s.at[zz, tt, u])
-
-    near = jnp.minimum(z, Z - 1 - z)
-    outward = jnp.where(z < Z - 1 - z, 1, -1)
-
-    def order(i):
-        sign = jnp.where(i % 2 == 1, 1, -1)
-        return jnp.where(i <= 2 * near, z + sign * ((i + 1) // 2), z + outward * (i - near))
 
     def relay_rows(i):
         nxt = order(i)
@@ -570,7 +582,7 @@
         def _():
             got(zin.at[Z, :, cols], rz_r.at[Z, j])
             mid[:, cols] = mid[:, cols] + zin[Z, :, cols].astype(F32)
-    out[...] = mid[...].astype(BF)
+    out[...] = mid[...]
 
     sent(lat.at[s], lo_s)
     sent(edge, e_s)
@@ -580,10 +592,18 @@
         for j in range(NB):
             sent(hpb.at[rows(tt), pl.ds(j * cw, cw)], hx_s.at[tt, j])
     for zz in range(Z):
+        part = lat.at[2 * zz + c, rows(t)]
+
+        @pl.when((zz <= z) & (z < Z - 1))
+        def _():
+            sent(part, lzr_s.at[zz])
+
+        @pl.when((zz >= z) & (z > 0))
+        def _():
+            sent(part, lzl_s.at[zz])
+
         @pl.when(zz != z)
         def _():
-            part = lat.at[2 * zz + c, rows(t)]
-            sent(part, lz_s.at[zz])
             for tt in xpart:
                 sent(part, lx_s.at[zz, tt])
             for tt in range(T):
@@ -675,14 +695,14 @@
         V(Z, 16, wmax, dtype=F32), V(Z, 16, wmax, dtype=F32), V(R, wmax),
         V(8, LANES) if share else V(Z, T, B, D), V(Z, T - 1, B, D), V(Z + 1, B, D),
         sem(8),
-        sem(Z), sem(Z), sem(Z, T), sem(Z, T), sem(Z, T), sem(Z, T), one, one,
+        sem(Z), sem(Z), sem(Z), sem(Z, T), sem(Z, T), sem(Z, T), sem(Z, T), one, one,
         sem(3, Z), sem(3, Z), sem(3, Z, G), sem(3, Z, G), sem(3), sem(3), sem(3),
         sem(T, 4), sem(T, 4), sem(Z, U), sem(Z, U), sem(Z, U), sem(Z, T, U), sem(Z, T, U), one, one,
         sem(Z, T, 2), sem(Z, T, 2), sem(Z, 2), sem(Z + 1, 2),
     ]
     return pl.pallas_call(
         functools.partial(layer_kernel, n),
-        out_shape=jax.ShapeDtypeStruct((B, D), BF),
+        out_shape=jax.ShapeDtypeStruct((B, D), F32),
         in_specs=[vmem] * 6 + [hbm] * 11,
         out_specs=vmem,
         scratch_shapes=scratch,
@@ -691,10 +711,10 @@
         ),
         name="layer",
     )(
-        latent, rope_key, query_wide, query_narrow, trig, norm_gain.reshape(1, D),
+        latent, rope_key.T, query_wide, query_narrow, trig, norm_gain.reshape(1, D),
         layer_input, key_up_wide, key_up_narrow, value_up_wide, value_up_narrow,
         out_wide, out_narrow, conv_weight, gate_weight, value_weight, down_weight,
-    )
+    ).astype(BF)
 
 
 def solution(mesh):

time: 147 us -> 141 us (0.959)
  Pallas kernels: 142 us -> 138 us
  local copies, waits for them, and re-layouts: 3.34 us -> 0.09 us
  other arithmetic: 1.13 us -> 3.06 us
    pallas_call x1, Pallas kernels: 142 us -> 138 us  [layer(): pl.pallas_call(functools.partial(layer_kernel, n), out_shape=jax.ShapeDty...]
    unnamed x2 -> x0, local copies, waits for them, and re-layouts: 3.25 us -> none
    convert_element_type x0 -> x1, other arithmetic: none -> 1.92 us  [layer(): return pl.pallas_call(functools.partial(layer_kernel, n), out_shape=jax.S...]
where the time goes in v2:
time: 141 us
  Pallas kernels  138 us (98%)
  other arithmetic  3.06 us (2%)
    pallas_call x1, Pallas kernels, layer(): pl.pallas_call(functools.partial(layer_kernel, n), out_shape=jax.ShapeDty...  138 us

profile of v2, /device:TPU:25, one launch (start us, length us, event | category | flops | bytes accessed | tf_op | source)
XLA Modules:
  0.0 140.9 jit_solution(10775612858266386617)
XLA Ops:
  0.0 0.1 mul.43
  0.1 0.4 multiply_cosine_fusion
  0.5 0.7 maximum_select_fusion.trig
  1.2 137.7 %layer.1 = f32[96,2048]{1,0:T(8,128)} custom-call(bf16[192,512]{1,0:T(8,128)(2,1)} %latent.1, bf16[64,192]{1,0:T(8,128)(2,1)} %bitcast.2, bf16[192,768]{1,0:T(8,128)(2,1)} %query_w.1, bf16[192,512]{1,0:T(8,128)(2,1)} %query_n.1, f32[2,192,128]{2,1,0:T(8,128)} %maximum_select_fusion.trig, f32[1,2048]{1,0:T(1,128)} %bitcast.3, bf16[96,2048]{1,0:T(8,128)(2,1)} %x_in.1, ...), custom_call_target="tpu_custom_call" | custom-call | tf_op jit(solution)/shard_map/layer/pallas_call | solution.py:703
  139.0 1.9 %convert_element_type.19 = bf16[96,2048]{1,0:T(8,128)(2,1)} convert(f32[96,2048]{1,0:T(8,128)} %layer.1) | non-fusion elementwise | flops 196608 | bytes 1179648 | tf_op jit(solution)/shard_map/convert_element_type | solution.py:717
  (4 shorter events, 0.0 us)

commit v3 on v2

--- a/solution.py
+++ b/solution.py
@@ -47,12 +47,12 @@
     out,
     lat, kuw_v, kun_v, vuw_v, vun_v, ow_v, xin_v,
     taps, qw, qn, kw, kn, vw, vn, att, hpb, hrecv, mid,
-    wg, wv, wd, xs, gp, vp, edge, halo, hid, pb, xr, zin,
+    wg, wv, wd, xs, gp, vp, edge, halo, hid, pb, xr, zin, acc, beside_in,
     loc,
     lzr_s, lzl_s, lz_r, lx_s, lx_r, lc_s, lc_r, lo_s, lo_r,
     wz_s, wz_r, wy_s, wy_r, wc_s, wc_r, wl,
     hx_s, hx_r, azr_s, azl_s, az_r, ax_s, ax_r, e_s, e_r,
-    rx_s, rx_r, rz_s, rz_r,
+    rx_s, rx_r, rz_s, rz_r, nb_s, nb_r,
 ):
     G, S, T = n["G"], n["S"], n["T"]
     Z = S // 2
@@ -444,10 +444,10 @@
     for u in range(U):
         forward(z, u)
     relay_y(1)
+    relay_core(0)
     if Z > 1:
         relay_rows(1)
     spread(2)
-    relay_core(0)
     arrive(0)
     relay_core(1)
     arrive(1)
@@ -475,7 +475,7 @@
         def _():
             relay_rows(i + 2)
 
-        @pl.when(i == max(0, Z - 3))
+        @pl.when(i == max(0, Z - 4))
         def _():
             relay_y(2)
         return carry
@@ -500,9 +500,44 @@
     SJ = S // J
     DJ = D // J
 
-    def summed(zi, j):
+    last = pl.ds((J - 1) * DJ, DJ)
+
+    def beside(zi):
+        return (zi == z - 1) | (zi == z + 1)
+
+    def cross(zi, j):
+        cols = pl.ds(j * DJ, DJ)
+        for tt in xpart:
+            rcopy(
+                pb.at[zi, tt, :, cols], xr.at[zi, slot(t, tt), :, cols],
+                rx_s.at[zi, tt, j], rx_r.at[zi, t, j], xdev(tt),
+            ).start()
+
+    def own_rows():
+        for tt in xpart:
+            for side, there in ((0, z > 0), (1, z < Z - 1)):
+                @pl.when(there)
+                def _():
+                    part = beside_in.at[side, slot(tt, t)]
+                    got(part, nb_r.at[side, tt])
+                    pb[z, tt, :, last] = (
+                        pb[z, tt, :, last].astype(F32) + part[...].astype(F32)
+                    ).astype(BF)
+        cross(z, J - 1)
+
+    def summed(zi, j, own=False):
         cols = pl.ds(j * DJ, DJ)
         total = pb[zi, t, :, cols].astype(F32)
+        if n["near"] and j == J - 1 and not own:
+            acc[...] = total
+
+            @pl.when(jnp.logical_not(beside(zi)))
+            def _():
+                for tt in xpart:
+                    part = xr.at[zi, slot(tt, t), :, cols]
+                    got(part, rx_r.at[zi, tt, j])
+                    acc[...] = acc[...] + part[...].astype(F32)
+            return acc[...]
         for tt in xpart:
             part = xr.at[zi, slot(tt, t), :, cols]
             got(part, rx_r.at[zi, tt, j])
@@ -552,18 +587,31 @@
             for b in range(j * SJ, j * SJ + SJ):
                 part = dot(hid[...], wd[b // 2, b % 2]).astype(BF)
                 pb[zi, :, :, pl.ds(b * OW, OW)] = part.reshape(T, B, OW)
-            cols = pl.ds(j * DJ, DJ)
-            for tt in xpart:
-                rcopy(
-                    pb.at[zi, tt, :, cols], xr.at[zi, slot(t, tt), :, cols],
-                    rx_s.at[zi, tt, j], rx_r.at[zi, t, j], xdev(tt),
-                ).start()
+            if n["near"] and j == J - 1:
+                @pl.when(jnp.logical_not(beside(zi)) & (zi != z))
+                def _():
+                    cross(zi, j)
+
+                @pl.when(beside(zi))
+                def _():
+                    side = jnp.where(zi < z, 1, 0)
+                    for tt in xpart:
+                        rcopy(
+                            pb.at[zi, tt, :, last], beside_in.at[side, slot(tt, t)],
+                            nb_s.at[side, tt], nb_r.at[side, tt], zdev(zi),
+                        ).start()
+            else:
+                cross(zi, j)
         return carry
 
     lax.fori_loop(0, Z, mix, 0)
 
     def pass_on(k, carry):
         zi = order(Z - 1 - k)
+        if n["near"]:
+            @pl.when(k == 1)
+            def _():
+                own_rows()
         for j in range(J):
             add_up(zi, j)
         return carry
@@ -571,7 +619,7 @@
     lax.fori_loop(0, Z - 1, pass_on, 0)
     for j in range(J):
         cols = pl.ds(j * DJ, DJ)
-        mid[:, cols] = mid[:, cols] + summed(z, j)
+        mid[:, cols] = mid[:, cols] + summed(z, j, own=True)
 
         @pl.when(z > 0)
         def _():
@@ -612,7 +660,18 @@
                 sent(pb.at[zz, t, :, pl.ds(j * DJ, DJ)], rz_s.at[zz, j])
         for tt in xpart:
             for j in range(J):
-                sent(pb.at[zz, tt, :, pl.ds(j * DJ, DJ)], rx_s.at[zz, tt, j])
+                if n["near"] and j == J - 1:
+                    @pl.when(jnp.logical_not(beside(zz)))
+                    def _():
+                        sent(pb.at[zz, tt, :, last], rx_s.at[zz, tt, j])
+                else:
+                    sent(pb.at[zz, tt, :, pl.ds(j * DJ, DJ)], rx_s.at[zz, tt, j])
+    if n["near"]:
+        for side, there in ((0, z < Z - 1), (1, z > 0)):
+            @pl.when(there)
+            def _():
+                for tt in xpart:
+                    sent(pb.at[z, tt, :, last], nb_s.at[side, tt])
     if not n["share"]:
         rows_sent()
 
@@ -661,8 +720,11 @@
     depth, ow = gate_weight.shape[0], down_weight.shape[1]
     U = 2 if B % 32 == 0 else 1
     share = Z * T * B * D * 2 > 8 << 20
+    near = not share and Z > 2
+    small = (B, D // 2) if near else (8, LANES)
     n = dict(
         share=share,
+        near=near,
         U=U,
         G=G,
         S=S,
@@ -694,11 +756,13 @@
         V(Z, T, B, D), V(Z, R, wmax), V(Z, R, wmax, dtype=BF if share else F32),
         V(Z, 16, wmax, dtype=F32), V(Z, 16, wmax, dtype=F32), V(R, wmax),
         V(8, LANES) if share else V(Z, T, B, D), V(Z, T - 1, B, D), V(Z + 1, B, D),
+        V(*small, dtype=F32), V(2, T - 1, *small),
         sem(8),
         sem(Z), sem(Z), sem(Z), sem(Z, T), sem(Z, T), sem(Z, T), sem(Z, T), one, one,
         sem(3, Z), sem(3, Z), sem(3, Z, G), sem(3, Z, G), sem(3), sem(3), sem(3),
         sem(T, 4), sem(T, 4), sem(Z, U), sem(Z, U), sem(Z, U), sem(Z, T, U), sem(Z, T, U), one, one,
         sem(Z, T, 2), sem(Z, T, 2), sem(Z, 2), sem(Z + 1, 2),
+        sem(2, T), sem(2, T),
     ]
     return pl.pallas_call(
         functools.partial(layer_kernel, n),

time: 141 us -> 137 us (0.972)
  Pallas kernels: 138 us -> 133 us
    pallas_call x1, Pallas kernels: 138 us -> 133 us  [layer(): pl.pallas_call(functools.partial(layer_kernel, n), out_shape=jax.ShapeDty...]
where the time goes in v3:
time: 137 us
  Pallas kernels  133 us (97%)
  other arithmetic  3.06 us (2%)
    pallas_call x1, Pallas kernels, layer(): pl.pallas_call(functools.partial(layer_kernel, n), out_shape=jax.ShapeDty...  133 us

profile of v3, /device:TPU:25, one launch (start us, length us, event | category | flops | bytes accessed | tf_op | source)
XLA Modules:
  0.0 136.6 jit_solution(14490173469666059413)
XLA Ops:
  0.0 0.1 mul.43
  0.1 0.4 multiply_cosine_fusion
  0.5 0.7 maximum_select_fusion.trig
  1.2 133.5 %layer.1 = f32[96,2048]{1,0:T(8,128)} custom-call(bf16[192,512]{1,0:T(8,128)(2,1)} %latent.1, bf16[64,192]{1,0:T(8,128)(2,1)} %bitcast.2, bf16[192,768]{1,0:T(8,128)(2,1)} %query_w.1, bf16[192,512]{1,0:T(8,128)(2,1)} %query_n.1, f32[2,192,128]{2,1,0:T(8,128)} %maximum_select_fusion.trig, f32[1,2048]{1,0:T(1,128)} %bitcast.3, bf16[96,2048]{1,0:T(8,128)(2,1)} %x_in.1, ...), custom_call_target="tpu_custom_call" | custom-call | tf_op jit(solution)/shard_map/layer/pallas_call | solution.py:767
  134.7 1.9 %convert_element_type.19 = bf16[96,2048]{1,0:T(8,128)(2,1)} convert(f32[96,2048]{1,0:T(8,128)} %layer.1) | non-fusion elementwise | flops 196608 | bytes 1179648 | tf_op jit(solution)/shard_map/convert_element_type | solution.py:781
  (4 shorter events, 0.0 us)
